TPU v7x, 1024 devices: a whole 8x8x8 slice. The times are simulated.
1024 devices in a mesh: tp: 64 (over z, y), dp: 16 (over x, core).
Axes of the slice: x: 8, y: 8, z: 8, core: 2. Of those that a mesh axis runs over, the one named last changes fastest.
Arguments:
- stream: bfloat16 [128, 4096], P('dp', 'tp'), may hold values from -6 to 6
- query_weight: bfloat16 [2, 4096, 3072], P(None, 'dp', 'tp'), may hold values from -0.09375 to 0.09375
- key_weight: bfloat16 [2, 4096, 3072], P(None, 'dp', 'tp'), may hold values from -0.09375 to 0.09375
- value_weight: bfloat16 [2, 4096, 3072], P(None, 'dp', 'tp'), may hold values from -0.09375 to 0.09375
- outgate_weight: bfloat16 [2, 4096, 3072], P(None, 'dp', 'tp'), may hold values from -0.09375 to 0.09375
- gate_weight: bfloat16 [2, 4096, 32], replicated, may hold values from -0.09375 to 0.09375
- gate_bias: float32 [2, 32], replicated, may hold values from -1 to 3
- output_weight: bfloat16 [2, 3072, 4096], P(None, 'dp', 'tp'), may hold values from -0.109375 to 0.109375
- norm_gain: float32 [2, 4096], replicated, may hold values from 0.1 to 1.9
- matrix_state: float32 [2, 128, 192, 16, 192], P(None, 'dp', 'tp'), may hold values from -0.6 to 0.6
- normalizer_state: float32 [2, 128, 16, 192], P(None, 'dp'), may hold values from -0.6 to 0.6
- stabilizer_state: float32 [2, 128, 16], P(None, 'dp'), may hold values from -4 to 4
Outputs:
- out_stream: bfloat16 [128, 4096], P('dp', 'tp')
- new_matrix: float32 [2, 128, 192, 16, 192], P(None, 'dp', 'tp')
- new_normalizer: float32 [2, 128, 16, 192], P(None, 'dp')
- new_stabilizer: float32 [2, 128, 16], P(None, 'dp')
All inputs are finite; a program needn't handle non-finite values.
Results may differ from a plain program's by a relative error of at most 0.015.
Values may be sent and summed in bfloat16 or wider, within the bound.
No kernel may reach another device: no remote copies, remote signals or barrier semaphores. Data moves between devices by JAX's collectives and lax.ppermute only.
A program may use at most 32 MiB of HBM per device.

v0:
```python
import functools

import jax
import jax.numpy as jnp
from jax import lax
from jax.experimental import pallas as pl
from jax.experimental.pallas import tpu as pltpu
from jax.sharding import PartitionSpec as P


residual_scale = 8.0**0.25
norm_eps = 1e-05
LANES = 128
MOST_VMEM = 67_043_328
F32 = jnp.float32


def exchange(pieces, axis):
    return lax.all_to_all(pieces, axis, split_axis=0, concat_axis=0, tiled=True)


def after(x, earlier):
    return lax.optimization_barrier((x, earlier))[0]


def step_of(held, bit):
    size = lax.axis_size("dp")
    return lax.ppermute(held, "dp", [(i, i ^ bit) for i in range(size)])


def merged(held, got):
    return lax.optimization_barrier(jnp.concatenate([held, got]))


def chain_order(size):
    held, bit = [0], size // 2
    while bit > 1:
        held = held + [h ^ bit for h in held]
        bit //= 2
    return held


def row_dot(x, turned):
    return lax.dot_general(x, turned, (((1,), (1,)), ((), ())), preferred_element_type=F32)


def blocks_dot(x_ref, halves, order, low=0, high=None):
    me = lax.axis_index("dp")
    rows = halves[0].shape[2]
    total = None
    for half, ref in enumerate(halves):
        for slot, other in enumerate(order):
            at = me ^ (other ^ half)
            if len(x_ref.shape) == 3:
                x = x_ref[at]
            else:
                x = x_ref[:, pl.ds(pl.multiple_of(at * rows, rows), rows)]
            product = row_dot(x, ref[slot, low:high, :])
            total = product if total is None else total + product
    return total


def pair_up(pieces_ref, width, at):
    two = [pieces_ref[2 * at + k][:, :width].astype(F32) for k in range(2)]
    return jnp.concatenate(two, axis=1)


def spread(ref, x):
    if x.shape[1] < LANES:
        x = jnp.concatenate([x, jnp.zeros((x.shape[0], LANES - x.shape[1]), x.dtype)], axis=1)
    x = x.astype(ref.dtype)
    for copy in range(ref.shape[0]):
        ref[copy] = x


def call(kernel, out_shape, *arrays, flops=10**6, scratch=(), specs=None, out_specs=None, aliases=None, room=32 * 2**20):
    moved = sum(a.size * a.dtype.itemsize for a in arrays)
    extra = {} if specs is None else {"in_specs": specs}
    if out_specs is not None:
        extra["grid"] = (1,)
    if out_specs is not None:
        extra["out_specs"] = out_specs
    return pl.pallas_call(
        kernel,
        out_shape=out_shape,
        scratch_shapes=list(scratch),
        input_output_aliases=aliases or {},
        cost_estimate=pl.CostEstimate(flops=flops, bytes_accessed=moved, transcendentals=0),
        compiler_params=pltpu.CompilerParams(vmem_limit_bytes=room),
        **extra,
    )(*arrays)


def one_block(shape, at=None):
    at = at or (0,) * len(shape)
    return pl.BlockSpec(shape, lambda step: at)


def pack_kernel(*refs):
    count = (len(refs) - 3) // 2
    given, (own_ref, chain_ref) = refs[:count], refs[count : count + 2]
    found, sems = refs[count + 2 : -1], refs[-1]
    fetches = [pltpu.make_async_copy(g, f, sems.at[k]) for k, (g, f) in enumerate(zip(given, found))]
    for fetch in fetches:
        fetch.start()
    for fetch in fetches:
        fetch.wait()
    *projections, output = found
    at = 0
    for ref in projections:
        size = ref.shape[1]
        own_ref[at : at + size, :] = ref[0]
        chain_ref[0, at : at + size, :] = ref[1]
        at += size
    blocks, size, rows = output.shape
    for block in range(blocks):
        chain_ref[0, at : at + size, :rows] = output[block]
        chain_ref[0, at : at + size, rows:] = jnp.zeros(
            (size, chain_ref.shape[2] - rows), chain_ref.dtype
        )
        at += size


def copies_kernel(x_ref, out_ref):
    spread(out_ref, x_ref[...].astype(F32))


def whole_kernel(pieces_ref, x_ref, cut_ref):
    width = x_ref.shape[1] // pieces_ref.shape[0]
    rows = cut_ref.shape[2]
    for at in range(pieces_ref.shape[0] // 2):
        low = 2 * width * at
        pair = pair_up(pieces_ref, width, at).astype(x_ref.dtype)
        x_ref[:, low : low + 2 * width] = pair
        cut_ref[low // rows, :, low % rows : low % rows + 2 * width] = pair


def partial_kernel(x_ref, weight_ref, out_ref):
    owners, seqs, rows = x_ref.shape
    x = x_ref[...].reshape(owners * seqs, rows)
    out = row_dot(x, weight_ref[...])
    out_ref[...] = out.reshape(out_ref.shape).astype(out_ref.dtype)


def sum_kernel(cut, parts_ref, qk_ref, vo_ref):
    out = sum(parts_ref[at].astype(F32) for at in range(parts_ref.shape[0]))
    spread(qk_ref, out[:, :cut])
    vo_ref[...] = out[:, cut:].astype(vo_ref.dtype)


def norm_kernel(cut, high, order, pieces_ref, gain_ref, held_ref, got_ref, x_ref, qk_ref, vo_ref):
    count, width = pieces_ref.shape[0], x_ref.shape[1] // pieces_ref.shape[0]
    pairs = [pair_up(pieces_ref, width, at) for at in range(count // 2)]
    features = x_ref.shape[1]
    mean = jnp.sum(sum(pairs), axis=1, keepdims=True) / features
    pairs = [p - mean for p in pairs]
    variance = jnp.sum(sum(p * p for p in pairs), axis=1, keepdims=True) / features
    scale = lax.rsqrt(variance + norm_eps)
    for at, p in enumerate(pairs):
        cols = slice(2 * width * at, 2 * width * (at + 1))
        x_ref[:, cols] = (p * scale * gain_ref[:, cols]).astype(x_ref.dtype)
    out = blocks_dot(x_ref, (held_ref, got_ref), order, 0, high)
    spread(qk_ref, out[:, :cut])
    vo_ref[...] = out[:, cut:].astype(vo_ref.dtype)


def head_sums(x, heads):
    x = x.reshape(heads, -1, *x.shape[1:]).sum(1)
    lane = lax.broadcasted_iota(jnp.int32, (x.shape[1], LANES), 1)
    sums = jnp.sum(x, axis=2, keepdims=True)
    total = jnp.zeros((x.shape[1], LANES), F32)
    for head in range(heads):
        total = jnp.where(lane == head, sums[head], total)
    return total


def side_pairs(x):
    return jnp.stack([jnp.concatenate([x[at], x[at + 1]], axis=1) for at in range(0, len(x), 2)])


def readout_kernel(scale, pieces_ref, vo_ref, retain_ref, admit_ref, state_ref, normalizer_ref, out_ref):
    heads = retain_ref.shape[1]
    width = vo_ref.shape[1] // 2
    both = pieces_ref[...].astype(F32)
    query = side_pairs(both[:, :, :width])
    key = side_pairs(both[:, :, width : 2 * width]) * scale
    retain, admit = retain_ref[...], admit_ref[...]
    of_key = head_sums(query * key, heads)[:, :heads] * admit
    of_normalizer = head_sums(query * normalizer_ref[...], heads)[:, :heads] * retain
    divisor = jnp.maximum(jnp.abs(of_normalizer + of_key), 1.0)
    vo = vo_ref[...].astype(F32)
    parts = []
    for e in range(state_ref.shape[0]):
        numerator = head_sums(query * state_ref[e], heads)[:, :heads] * retain
        value = vo[:, e * heads : (e + 1) * heads]
        gate = vo[:, width + e * heads : width + (e + 1) * heads]
        parts.append((numerator + value * of_key) / divisor * jax.nn.sigmoid(gate))
    spread(out_ref, jnp.concatenate(parts, axis=1))


def branch_kernel(width, low, high, order, pieces_ref, x_ref, held_ref, got_ref, out_ref, wide_ref):
    blocks, seqs, rows = wide_ref.shape
    count = pieces_ref.shape[0] // blocks
    for at in range(blocks):
        found = [pieces_ref[count * at + k][:, :width].astype(F32) for k in range(count)]
        found.append(jnp.zeros((seqs, rows - count * width), F32))
        wide_ref[at] = jnp.concatenate(found, axis=1).astype(wide_ref.dtype)
    branch = blocks_dot(wide_ref, (held_ref, got_ref), order, low, high)
    spread(out_ref, residual_scale * x_ref[...].astype(F32) + branch)


def last_kernel(features, pieces_ref, gain_ref, out_ref):
    width = out_ref.shape[1]
    pieces = [pieces_ref[at].astype(F32) for at in range(pieces_ref.shape[0])]
    mean = jnp.sum(sum(pieces), axis=1, keepdims=True) / features
    lane = lax.broadcasted_iota(jnp.int32, pieces[0].shape, 1)
    off = [jnp.where(lane < width, p - mean, 0.0) for p in pieces]
    variance = jnp.sum(sum(p * p for p in off), axis=1, keepdims=True) / features
    own = pieces_ref[lax.axis_index("tp")].astype(F32)[:, :width]
    out = (own - mean) * lax.rsqrt(variance + norm_eps) * gain_ref[...]
    out_ref[...] = out.astype(out_ref.dtype)


def column(row, heads):
    at = lax.broadcasted_iota(jnp.int32, (heads, heads), 0)
    lane = lax.broadcasted_iota(jnp.int32, (heads, heads), 1)
    wide = jnp.broadcast_to(row, (heads, heads))
    return jnp.sum(jnp.where(at == lane, wide, 0.0), axis=1, keepdims=True)


def update_kernel(scale, parts, *refs):
    pieces_ref, vo_ref, retain_ref, admit_ref, state_ref, normalizer_ref = refs[:6]
    new_state_ref, new_normalizer_ref, rows_ref = refs[-3:]
    _, seqs, channels, heads, size = state_ref.shape
    width = size // parts
    rows_ref[...] = pieces_ref[...].astype(F32).reshape(rows_ref.shape)
    vo = vo_ref[...].astype(F32)
    for seq in range(seqs):
        found = [
            rows_ref[pl.ds(seq + seqs * part, heads, stride=seqs * parts), :]
            for part in range(parts)
        ]
        key = jnp.concatenate([f[:, width : 2 * width] for f in found], axis=1) * scale
        retain = column(retain_ref[seq : seq + 1, :], heads)
        admit = column(admit_ref[seq : seq + 1, :], heads)
        new_normalizer_ref[0, seq] = retain * normalizer_ref[0, seq] + admit * key
        for e in range(channels):
            value = column(vo[seq : seq + 1, e * heads : (e + 1) * heads], heads)
            new_state_ref[0, seq, e] = retain * state_ref[0, seq, e] + (admit * value) * key


def update(block_no, saved, state, normalizer, made):
    size, width = state.shape[4], saved[1].shape[1] // 2
    blocks = [
        one_block((1, *x.shape[1:]), (block_no,) + (0,) * (x.ndim - 1)) for x in (state, normalizer)
    ]
    whole = [one_block(x.shape) for x in saved]
    arrays = (*saved, state, normalizer, *made)
    return call(
        functools.partial(update_kernel, size**-0.5, size // width),
        [jax.ShapeDtypeStruct(x.shape, x.dtype) for x in (state, normalizer)],
        *arrays,
        scratch=[pltpu.VMEM((saved[0].shape[0] * saved[0].shape[1], LANES), F32)],
        specs=[*whole, *blocks, *[pl.BlockSpec(memory_space=pl.ANY) for _ in made]],
        out_specs=blocks,
        aliases={6: 0, 7: 1} if made else None,
        room=MOST_VMEM - 400 * 2**10,
    )


def shards(
    stream,
    query_weight,
    key_weight,
    value_weight,
    outgate_weight,
    gate_weight,
    gate_bias,
    output_weight,
    norm_gain,
    matrix_state,
    normalizer_state,
    stabilizer_state,
):
    head_count = gate_bias.shape[1] // 2
    head_size = normalizer_state.shape[3]
    seqs, feats = stream.shape
    rows, cols = query_weight.shape[1:]
    peers = lax.axis_size("tp")
    owners = lax.axis_size("dp")
    order = chain_order(owners)
    me = lax.axis_index("tp")
    bf16 = stream.dtype
    copies = jax.ShapeDtypeStruct((peers, seqs, LANES), bf16)
    pair = jax.ShapeDtypeStruct((seqs, 2 * cols), bf16)
    pair_cols = 2 * cols
    per_head = head_size // pair_cols
    turned = [jnp.swapaxes(w, 1, 2) for w in (query_weight, key_weight, value_weight, outgate_weight)]
    out_turned = jnp.swapaxes(output_weight, 1, 2)
    held_in = pl.BlockSpec(memory_space=pltpu.MemorySpace.HBM)
    given = (*turned, out_turned)
    own, chain = call(
        pack_kernel,
        (
            jax.ShapeDtypeStruct((4 * cols, rows), bf16),
            jax.ShapeDtypeStruct((1, 4 * cols + 2 * feats, rows), bf16),
        ),
        *given,
        specs=[held_in] * len(given),
        scratch=[*[pltpu.VMEM(w.shape, bf16) for w in given], pltpu.SemaphoreType.DMA((len(given),))],
        room=MOST_VMEM - 160 * 2**10,
    )

    def by_piece(x):
        x = x.reshape(*x.shape[:-1], per_head, pair_cols)
        return jnp.moveaxis(x, 0, -2).reshape(*x.shape[1:-3], peers // 2, seqs, pair_cols)

    whole_x = jax.ShapeDtypeStruct((seqs, peers * feats), bf16)
    pieces = exchange(call(copies_kernel, copies, stream), "tp")
    got = step_of(chain, 8)
    x_local = stream
    x_full, cut = call(
        whole_kernel, (whole_x, jax.ShapeDtypeStruct((owners, seqs, rows), bf16)), pieces
    )
    seen = after((matrix_state, normalizer_state), cut)
    states = [by_piece(m) for m in seen[0]]
    normalizers = [by_piece(n) for n in seen[1]]
    everyone = exchange(cut, "dp")
    partial = call(
        partial_kernel, jax.ShapeDtypeStruct((owners, seqs, 4 * cols), bf16), everyone, own
    )
    partial = after(partial, (states, normalizers))
    parts = exchange(partial, "dp")
    chain = merged(after(chain, (partial,)), got)
    got = step_of(chain, 4)
    saved, new_stabs = ([], [])
    for block_no in range(gate_bias.shape[0]):
        if block_no == 0:
            qk, vo = call(functools.partial(sum_kernel, 2 * cols), (copies, pair), parts)
            chain = merged(after(chain, (qk,)), got)
            got = step_of(chain, 2)
        else:
            x_full, qk, vo = call(
                functools.partial(norm_kernel, 2 * cols, 4 * cols, order),
                (whole_x, copies, pair),
                pieces,
                norm_gain[:1],
                chain,
                got,
            )
            x_local = lax.dynamic_slice_in_dim(x_full, me * feats, feats, 1)
            tied = after(saved[0], (qk,))
            made = update(0, tied, matrix_state, normalizer_state, ())
        pieces = exchange(qk, "tp")
        gate_pre = (
            jnp.dot(x_full, gate_weight[block_no], preferred_element_type=F32)
            + gate_bias[block_no]
        )
        log_in = gate_pre[:, :head_count]
        log_forget = jax.nn.log_sigmoid(gate_pre[:, head_count:])
        old_stab = stabilizer_state[block_no]
        stab_new = jnp.maximum(log_forget + old_stab, log_in)
        retain = jnp.exp(log_forget + old_stab - stab_new)
        admit = jnp.exp(log_in - stab_new)
        hidden = call(
            functools.partial(readout_kernel, head_size**-0.5),
            copies,
            pieces,
            vo,
            retain,
            admit,
            states[block_no],
            normalizers[block_no],
        )
        if block_no == 0:
            chain = merged(after(chain, (hidden,)), got)
            got = step_of(chain, 1)
        saved.append((pieces, vo, retain, admit))
        pieces = exchange(hidden, "tp")
        low = 4 * cols + block_no * feats
        summed = call(
            functools.partial(branch_kernel, cols, low, low + feats, order),
            copies,
            pieces,
            x_local,
            chain,
            got,
            scratch=[pltpu.VMEM((owners, seqs, rows), bf16)],
        )
        new_stabs.append(stab_new)
        pieces = exchange(summed, "tp")
    gain = lax.dynamic_slice_in_dim(norm_gain[1:], me * feats, feats, 1)
    out = call(
        functools.partial(last_kernel, peers * feats),
        jax.ShapeDtypeStruct((seqs, feats), bf16),
        pieces,
        gain,
    )
    made = update(1, after(saved[1], (summed,)), matrix_state, normalizer_state, made)
    return (out, *made, jnp.stack(new_stabs))


def solution(mesh):
    return jax.shard_map(
        shards,
        mesh=mesh,
        in_specs=(
            P("dp", "tp"),
            P(None, "dp", "tp"),
            P(None, "dp", "tp"),
            P(None, "dp", "tp"),
            P(None, "dp", "tp"),
            P(),
            P(),
            P(None, "dp", "tp"),
            P(),
            P(None, "dp", "tp", None, None),
            P(None, "dp", None, None),
            P(None, "dp", None),
        ),
        out_specs=(
            P("dp", "tp"),
            P(None, "dp", "tp", None, None),
            P(None, "dp", None, None),
            P(None, "dp", None),
        ),
        check_vma=False,
    )
```

profile of v0, /device:TPU:2, one launch (start us, length us, event | category | flops | bytes accessed | tf_op | source)
XLA Modules:
  0.0 191.1 jit_solution(7796109135231615091)
XLA Ops:
  2.0 23.4 %all-to-all-start = ((bf16[64,8,128]{2,1,0:T(8,128)(2,1)}), bf16[64,8,128]{2,1,0:T(8,128)(2,1)S(1)}, u32[]{:S(2)}, u32[]{:S(2)}) async-start(bf16[64,8,128]{2,1,0:T(8,128)(2,1)} %shard_map.147), calls=%async_computation | async-start | bytes 262144 | tf_op jit(solution)/shard_map/all_to_all | solution.py:19
  25.4 1.7 shard_map.149
  27.1 6.6 %collective-permute-start = (bf16[1,320,256]{2,1,0:T(8,128)(2,1)}, bf16[1,320,256]{2,1,0:T(8,128)(2,1)S(1)}, u32[]{:S(2)}, u32[]{:S(2)}) collective-permute-start(bf16[1,320,256]{2,1,0:T(8,128)(2,1)} %get-tuple-element.40), channel_id=1, source_target_pairs={{0,8},{1,9},{2,10},{3,11},{4,12},{5,13},{6,14},{7,15},{8,0},{9,1},... | collective-permute-start | bytes 491528 | tf_op jit(solution)/shard_map/ppermute | solution.py:28
  33.8 4.3 %all-to-all-done.pieces_ref = bf16[64,8,128]{2,1,0:T(8,128)(2,1)S(1)} async-done(((bf16[64,8,128]{2,1,0:T(8,128)(2,1)}), bf16[64,8,128]{2,1,0:T(8,128)(2,1)S(1)}, u32[]{:S(2)}, u32[]{:S(2)}) %all-to-all-start) | async-done | bytes 131104 | tf_op jit(solution)/shard_map/all_to_all | solution.py:19
  38.1 0.7 shard_map.148
  38.8 7.3 %all-to-all-start.1 = ((bf16[16,8,256]{2,1,0:T(8,128)(2,1)}), bf16[16,8,256]{2,1,0:T(8,128)(2,1)S(1)}, u32[]{:S(2)}, u32[]{:S(2)}) async-start(bf16[16,8,256]{2,1,0:T(8,128)(2,1)} %get-tuple-element.31), calls=%async_computation.1 | async-start | bytes 131072 | tf_op jit(solution)/shard_map/all_to_all | solution.py:19
  46.1 1.2 fusion.10
  48.9 3.8 %all-to-all-done.1.x_ref = bf16[16,8,256]{2,1,0:T(8,128)(2,1)S(1)} async-done(((bf16[16,8,256]{2,1,0:T(8,128)(2,1)}), bf16[16,8,256]{2,1,0:T(8,128)(2,1)S(1)}, u32[]{:S(2)}, u32[]{:S(2)}) %all-to-all-start.1) | async-done | bytes 65568 | tf_op jit(solution)/shard_map/all_to_all | solution.py:19
  52.9 2.7 %collective-permute-start.1 = (bf16[2,320,256]{2,1,0:T(8,128)(2,1)S(1)}, bf16[2,320,256]{2,1,0:T(8,128)(2,1)S(1)}, u32[]{:S(2)}, u32[]{:S(2)}) collective-permute-start(bf16[2,320,256]{2,1,0:T(8,128)(2,1)S(1)} %pad_maximum_fusion.2), channel_id=1, source_target_pairs={{0,4},{1,5},{2,6},{3,7},{4,0},{5,1},{6,2},{7,3},{8,12},{9,13},{10,... | collective-permute-start | bytes 983048 | tf_op jit(solution)/shard_map/ppermute | solution.py:28
  55.6 18.3 %all_to_all.45.parts_ref = bf16[16,8,192]{2,1,0:T(8,128)(2,1)S(1)} all-to-all(bf16[16,8,192]{2,1,0:T(8,128)(2,1)S(1)} %shard_map.150), channel_id=1, replica_groups=mesh['tp'=64,'dp'=16] {'dp'}, dimensions={0} | all-to-all | bytes 98304 | tf_op jit(solution)/shard_map/all_to_all | solution.py:19
  74.7 3.3 %collective-permute-start.2 = (bf16[4,320,256]{2,1,0:T(8,128)(2,1)S(1)}, bf16[4,320,256]{2,1,0:T(8,128)(2,1)S(1)}, u32[]{:S(2)}, u32[]{:S(2)}) collective-permute-start(bf16[4,320,256]{2,1,0:T(8,128)(2,1)S(1)} %pad_maximum_fusion.1), channel_id=1, source_target_pairs={{0,2},{1,3},{2,0},{3,1},{4,6},{5,7},{6,4},{7,5},{8,10},{9,11},{10,... | collective-permute-start | bytes 1966088 | tf_op jit(solution)/shard_map/ppermute | solution.py:28
  78.0 5.8 %all-to-all-start.3 = ((bf16[64,8,128]{2,1,0:T(8,128)(2,1)}), bf16[64,8,128]{2,1,0:T(8,128)(2,1)S(1)}, u32[]{:S(2)}, u32[]{:S(2)}) async-start(bf16[64,8,128]{2,1,0:T(8,128)(2,1)} %get-tuple-element.36), calls=%async_computation.3 | async-start | bytes 262144 | tf_op jit(solution)/shard_map/all_to_all | solution.py:19
  83.8 1.1 convolution_add_fusion.1
  85.0 11.5 %all-to-all-done.3.pieces_ref.refs_0_ = bf16[64,8,128]{2,1,0:T(8,128)(2,1)S(1)} async-done(((bf16[64,8,128]{2,1,0:T(8,128)(2,1)}), bf16[64,8,128]{2,1,0:T(8,128)(2,1)S(1)}, u32[]{:S(2)}, u32[]{:S(2)}) %all-to-all-start.3) | async-done | bytes 131104 | tf_op jit(solution)/shard_map/all_to_all | solution.py:19
  97.2 1.9 collective-permute-start.3
  99.1 17.3 %all_to_all.46.pieces_ref = bf16[64,8,128]{2,1,0:T(8,128)(2,1)S(1)} all-to-all(bf16[64,8,128]{2,1,0:T(8,128)(2,1)S(1)} %shard_map.152), channel_id=1, replica_groups=mesh['tp'=64,'dp'=16] {'tp'}, dimensions={0} | all-to-all | bytes 262144 | tf_op jit(solution)/shard_map/all_to_all | solution.py:19
  116.4 1.0 shard_map.153
  117.4 4.6 %all-to-all-start.5 = ((bf16[64,8,128]{2,1,0:T(8,128)(2,1)}), bf16[64,8,128]{2,1,0:T(8,128)(2,1)S(1)}, u32[]{:S(2)}, u32[]{:S(2)}) async-start(bf16[64,8,128]{2,1,0:T(8,128)(2,1)} %shard_map.153), calls=%async_computation.5 | async-start | bytes 262144 | tf_op jit(solution)/shard_map/all_to_all | solution.py:19
  122.0 12.7 %all-to-all-done.5.pieces_ref = bf16[64,8,128]{2,1,0:T(8,128)(2,1)S(1)} async-done(((bf16[64,8,128]{2,1,0:T(8,128)(2,1)}), bf16[64,8,128]{2,1,0:T(8,128)(2,1)S(1)}, u32[]{:S(2)}, u32[]{:S(2)}) %all-to-all-start.5) | async-done | bytes 131104 | tf_op jit(solution)/shard_map/all_to_all | solution.py:19
  134.8 1.5 shard_map.154
  136.2 4.6 %all-to-all-start.6 = ((bf16[64,8,128]{2,1,0:T(8,128)(2,1)}), bf16[64,8,128]{2,1,0:T(8,128)(2,1)S(1)}, u32[]{:S(2)}, u32[]{:S(2)}) async-start(bf16[64,8,128]{2,1,0:T(8,128)(2,1)} %get-tuple-element.43), calls=%async_computation.6 | async-start | bytes 262144 | tf_op jit(solution)/shard_map/all_to_all | solution.py:19
  140.8 1.1 convolution_add_fusion
  142.1 11.5 %all-to-all-done.6.pieces_ref.refs_0_ = bf16[64,8,128]{2,1,0:T(8,128)(2,1)S(1)} async-done(((bf16[64,8,128]{2,1,0:T(8,128)(2,1)}), bf16[64,8,128]{2,1,0:T(8,128)(2,1)S(1)}, u32[]{:S(2)}, u32[]{:S(2)}) %all-to-all-start.6) | async-done | bytes 131104 | tf_op jit(solution)/shard_map/all_to_all | solution.py:19
  153.6 1.1 shard_map.155
  154.6 4.6 %all-to-all-start.7 = ((bf16[64,8,128]{2,1,0:T(8,128)(2,1)}), bf16[64,8,128]{2,1,0:T(8,128)(2,1)S(1)}, u32[]{:S(2)}, u32[]{:S(2)}) async-start(bf16[64,8,128]{2,1,0:T(8,128)(2,1)} %shard_map.155), calls=%async_computation.7 | async-start | bytes 262144 | tf_op jit(solution)/shard_map/all_to_all | solution.py:19
  159.3 12.6 %all-to-all-done.7.pieces_ref = bf16[64,8,128]{2,1,0:T(8,128)(2,1)S(1)} async-done(((bf16[64,8,128]{2,1,0:T(8,128)(2,1)}), bf16[64,8,128]{2,1,0:T(8,128)(2,1)S(1)}, u32[]{:S(2)}, u32[]{:S(2)}) %all-to-all-start.7) | async-done | bytes 131104 | tf_op jit(solution)/shard_map/all_to_all | solution.py:19
  171.9 1.0 shard_map.156
  172.9 4.6 %all-to-all-start.8 = ((bf16[64,8,128]{2,1,0:T(8,128)(2,1)}), bf16[64,8,128]{2,1,0:T(8,128)(2,1)S(1)}, u32[]{:S(2)}, u32[]{:S(2)}) async-start(bf16[64,8,128]{2,1,0:T(8,128)(2,1)} %shard_map.156), calls=%async_computation.8 | async-start | bytes 262144 | tf_op jit(solution)/shard_map/all_to_all | solution.py:19
  177.6 3.3 %shard_map.158 = (f32[2,8,3,16,192]{4,3,2,1,0:T(8,128)}, f32[2,8,16,192]{3,2,1,0:T(8,128)}) custom-call(bf16[64,8,128]{2,1,0:T(8,128)(2,1)} %copy-done, bf16[8,96]{1,0:T(8,128)(2,1)} %copy-done.9, f32[8,16]{1,0:T(8,128)} %copy-done.4, f32[8,16]{1,0:T(8,128)} %copy-done.3, f32[2,8,3,16,192]{4,3,2,1,0:T(8,128)} %refs_4_.3, f32[2,8,16,192]{3,2,1,0:T(8,128)} %refs_5_.3), custom_call_target="tpu_custom_call" | custom-call | flops 1000000 | bytes 920064 | tf_op jit(solution)/shard_map/pallas_call | solution.py:83
  181.6 3.3 %shard_map.159 = (f32[2,8,3,16,192]{4,3,2,1,0:T(8,128)}, f32[2,8,16,192]{3,2,1,0:T(8,128)}) custom-call(bf16[64,8,128]{2,1,0:T(8,128)(2,1)} %copy-done.1, bf16[8,96]{1,0:T(8,128)(2,1)} %copy-done.10, f32[8,16]{1,0:T(8,128)} %copy-done.6, f32[8,16]{1,0:T(8,128)} %copy-done.5, ...), custom_call_target="tpu_custom_call", output_to_operand_aliasing={{0}: (6, {}), {1}: (7, {})} | custom-call | flops 1000000 | bytes 1706496 | tf_op jit(solution)/shard_map/pallas_call | solution.py:83
  184.9 5.4 %all-to-all-done.8.pieces_ref = bf16[64,8,128]{2,1,0:T(8,128)(2,1)S(1)} async-done(((bf16[64,8,128]{2,1,0:T(8,128)(2,1)}), bf16[64,8,128]{2,1,0:T(8,128)(2,1)S(1)}, u32[]{:S(2)}, u32[]{:S(2)}) %all-to-all-start.8) | async-done | bytes 131104 | tf_op jit(solution)/shard_map/all_to_all | solution.py:19
  190.3 0.9 shard_map.157
  (59 shorter events, 5.4 us)
Async XLA Ops:
  0.6 0.7 copy-start.7
  2.0 36.1 %all-to-all-start = ((bf16[64,8,128]{2,1,0:T(8,128)(2,1)}), bf16[64,8,128]{2,1,0:T(8,128)(2,1)S(1)}, u32[]{:S(2)}, u32[]{:S(2)}) async-start(bf16[64,8,128]{2,1,0:T(8,128)(2,1)} %shard_map.147), calls=%async_computation | async-start | bytes 262144 | tf_op jit(solution)/shard_map/all_to_all | solution.py:19
  27.1 20.2 %copy-start.11 = (f32[2,8,16,192]{3,2,1,0:T(8,128)S(1)}, f32[2,8,16,192]{3,2,1,0:T(8,128)}, u32[]{:S(2)}) copy-start(f32[2,8,16,192]{3,2,1,0:T(8,128)} %refs_5_.3) | copy-start | bytes 589828
  27.1 25.7 %collective-permute-start = (bf16[1,320,256]{2,1,0:T(8,128)(2,1)}, bf16[1,320,256]{2,1,0:T(8,128)(2,1)S(1)}, u32[]{:S(2)}, u32[]{:S(2)}) collective-permute-start(bf16[1,320,256]{2,1,0:T(8,128)(2,1)} %get-tuple-element.40), channel_id=1, source_target_pairs={{0,8},{1,9},{2,10},{3,11},{4,12},{5,13},{6,14},{7,15},{8,0},{9,1},... | collective-permute-start | bytes 491528 | tf_op jit(solution)/shard_map/ppermute | solution.py:28
  38.8 13.8 %all-to-all-start.1 = ((bf16[16,8,256]{2,1,0:T(8,128)(2,1)}), bf16[16,8,256]{2,1,0:T(8,128)(2,1)S(1)}, u32[]{:S(2)}, u32[]{:S(2)}) async-start(bf16[16,8,256]{2,1,0:T(8,128)(2,1)} %get-tuple-element.31), calls=%async_computation.1 | async-start | bytes 131072 | tf_op jit(solution)/shard_map/all_to_all | solution.py:19
  48.1 4.6 %copy-start.2 = (bf16[192,256]{1,0:T(8,128)(2,1)S(1)}, bf16[192,256]{1,0:T(8,128)(2,1)}, u32[]{:S(2)}) copy-start(bf16[192,256]{1,0:T(8,128)(2,1)} %get-tuple-element.32.weight_ref) | copy-start | bytes 294916
  48.1 4.8 %copy-start.12 = (bf16[1,320,256]{2,1,0:T(8,128)(2,1)S(1)}, bf16[1,320,256]{2,1,0:T(8,128)(2,1)}, u32[]{:S(2)}) copy-start(bf16[1,320,256]{2,1,0:T(8,128)(2,1)} %get-tuple-element.40) | copy-start | bytes 491524
  48.9 29.1 %copy-start.15 = (f32[2,32]{1,0:T(2,128)S(1)}, f32[2,32]{1,0:T(2,128)}, u32[]{:S(2)}) copy-start(f32[2,32]{1,0:T(2,128)} %param.18) | copy-start | bytes 772
  52.8 32.1 %copy-start.14 = (f32[2,8,16]{2,1,0:T(8,128)S(1)}, f32[2,8,16]{2,1,0:T(8,128)}, u32[]{:S(2)}) copy-start(f32[2,8,16]{2,1,0:T(8,128)} %param.23) | copy-start | bytes 3076
  52.9 21.7 %collective-permute-start.1 = (bf16[2,320,256]{2,1,0:T(8,128)(2,1)S(1)}, bf16[2,320,256]{2,1,0:T(8,128)(2,1)S(1)}, u32[]{:S(2)}, u32[]{:S(2)}) collective-permute-start(bf16[2,320,256]{2,1,0:T(8,128)(2,1)S(1)} %pad_maximum_fusion.2), channel_id=1, source_target_pairs={{0,4},{1,5},{2,6},{3,7},{4,0},{5,1},{6,2},{7,3},{8,12},{9,13},{10,... | collective-permute-start | bytes 983048 | tf_op jit(solution)/shard_map/ppermute | solution.py:28
  74.6 22.3 %copy-start.9 = (bf16[8,96]{1,0:T(8,128)(2,1)}, bf16[8,96]{1,0:T(8,128)(2,1)S(1)}, u32[]{:S(2)}) copy-start(bf16[8,96]{1,0:T(8,128)(2,1)S(1)} %get-tuple-element.51.vo_ref.refs_1_) | copy-start | bytes 4612
  74.7 22.3 %collective-permute-start.2 = (bf16[4,320,256]{2,1,0:T(8,128)(2,1)S(1)}, bf16[4,320,256]{2,1,0:T(8,128)(2,1)S(1)}, u32[]{:S(2)}, u32[]{:S(2)}) collective-permute-start(bf16[4,320,256]{2,1,0:T(8,128)(2,1)S(1)} %pad_maximum_fusion.1), channel_id=1, source_target_pairs={{0,2},{1,3},{2,0},{3,1},{4,6},{5,7},{6,4},{7,5},{8,10},{9,11},{10,... | collective-permute-start | bytes 1966088 | tf_op jit(solution)/shard_map/ppermute | solution.py:28
  78.0 18.5 %all-to-all-start.3 = ((bf16[64,8,128]{2,1,0:T(8,128)(2,1)}), bf16[64,8,128]{2,1,0:T(8,128)(2,1)S(1)}, u32[]{:S(2)}, u32[]{:S(2)}) async-start(bf16[64,8,128]{2,1,0:T(8,128)(2,1)} %get-tuple-element.36), calls=%async_computation.3 | async-start | bytes 262144 | tf_op jit(solution)/shard_map/all_to_all | solution.py:19
  85.0 12.0 %copy-start.3 = (f32[8,16]{1,0:T(8,128)}, f32[8,16]{1,0:T(8,128)S(1)}, u32[]{:S(2)}) copy-start(f32[8,16]{1,0:T(8,128)S(1)} %get-tuple-element.53.admit_ref.refs_3_) | copy-start | bytes 1540
  85.0 12.0 %copy-start.4 = (f32[8,16]{1,0:T(8,128)}, f32[8,16]{1,0:T(8,128)S(1)}, u32[]{:S(2)}) copy-start(f32[8,16]{1,0:T(8,128)S(1)} %get-tuple-element.52.retain_ref.refs_2_) | copy-start | bytes 1540
  96.5 0.7 copy-start
  96.9 19.4 %copy-start.8 = (bf16[8,64]{1,0:T(8,128)(2,1)S(1)}, bf16[8,64]{1,0:T(8,128)(2,1)}, u32[]{:S(2)}) copy-start(bf16[8,64]{1,0:T(8,128)(2,1)} %x_ref.3) | copy-start | bytes 3076
  97.2 19.2 %collective-permute-start.3 = (bf16[8,320,256]{2,1,0:T(8,128)(2,1)S(1)}, bf16[8,320,256]{2,1,0:T(8,128)(2,1)S(1)}, u32[]{:S(2)}, u32[]{:S(2)}) collective-permute-start(bf16[8,320,256]{2,1,0:T(8,128)(2,1)S(1)} %pad_maximum_fusion.held_ref), channel_id=1, source_target_pairs={{0,1},{1,0},{2,3},{3,2},{4,5},{5,4},{6,7},{7,6},{8,9},{9,8},{10,11... | collective-permute-start | bytes 3932168 | tf_op jit(solution)/shard_map/ppermute | solution.py:28
  116.4 5.6 %copy-start.13 = (f32[2,4096]{1,0:T(2,128)S(1)}, f32[2,4096]{1,0:T(2,128)}, u32[]{:S(2)}) copy-start(f32[2,4096]{1,0:T(2,128)} %param.20) | copy-start | bytes 98308
  117.4 17.4 %all-to-all-start.5 = ((bf16[64,8,128]{2,1,0:T(8,128)(2,1)}), bf16[64,8,128]{2,1,0:T(8,128)(2,1)S(1)}, u32[]{:S(2)}, u32[]{:S(2)}) async-start(bf16[64,8,128]{2,1,0:T(8,128)(2,1)} %shard_map.153), calls=%async_computation.5 | async-start | bytes 262144 | tf_op jit(solution)/shard_map/all_to_all | solution.py:19
  136.2 36.7 %copy-start.10 = (bf16[8,96]{1,0:T(8,128)(2,1)}, bf16[8,96]{1,0:T(8,128)(2,1)S(1)}, u32[]{:S(2)}) copy-start(bf16[8,96]{1,0:T(8,128)(2,1)S(1)} %get-tuple-element.47.vo_ref.refs_1_) | copy-start | bytes 4612
  136.2 17.4 %all-to-all-start.6 = ((bf16[64,8,128]{2,1,0:T(8,128)(2,1)}), bf16[64,8,128]{2,1,0:T(8,128)(2,1)S(1)}, u32[]{:S(2)}, u32[]{:S(2)}) async-start(bf16[64,8,128]{2,1,0:T(8,128)(2,1)} %get-tuple-element.43), calls=%async_computation.6 | async-start | bytes 262144 | tf_op jit(solution)/shard_map/all_to_all | solution.py:19
  142.1 30.9 %copy-start.5 = (f32[8,16]{1,0:T(8,128)}, f32[8,16]{1,0:T(8,128)S(1)}, u32[]{:S(2)}) copy-start(f32[8,16]{1,0:T(8,128)S(1)} %get-tuple-element.49.admit_ref.refs_3_) | copy-start | bytes 1540
  142.1 30.9 %copy-start.6 = (f32[8,16]{1,0:T(8,128)}, f32[8,16]{1,0:T(8,128)S(1)}, u32[]{:S(2)}) copy-start(f32[8,16]{1,0:T(8,128)S(1)} %get-tuple-element.48.retain_ref.refs_2_) | copy-start | bytes 1540
  153.6 19.4 %copy-start.1 = (bf16[64,8,128]{2,1,0:T(8,128)(2,1)}, bf16[64,8,128]{2,1,0:T(8,128)(2,1)S(1)}, u32[]{:S(2)}) copy-start(bf16[64,8,128]{2,1,0:T(8,128)(2,1)S(1)} %all-to-all-done.6.pieces_ref.refs_0_) | copy-start | bytes 393220
  154.6 17.3 %all-to-all-start.7 = ((bf16[64,8,128]{2,1,0:T(8,128)(2,1)}), bf16[64,8,128]{2,1,0:T(8,128)(2,1)S(1)}, u32[]{:S(2)}, u32[]{:S(2)}) async-start(bf16[64,8,128]{2,1,0:T(8,128)(2,1)} %shard_map.155), calls=%async_computation.7 | async-start | bytes 262144 | tf_op jit(solution)/shard_map/all_to_all | solution.py:19
  172.9 17.3 %all-to-all-start.8 = ((bf16[64,8,128]{2,1,0:T(8,128)(2,1)}), bf16[64,8,128]{2,1,0:T(8,128)(2,1)S(1)}, u32[]{:S(2)}, u32[]{:S(2)}) async-start(bf16[64,8,128]{2,1,0:T(8,128)(2,1)} %shard_map.156), calls=%async_computation.8 | async-start | bytes 262144 | tf_op jit(solution)/shard_map/all_to_all | solution.py:19
where the time goes:
time: 192 us; the launch traced here: 191 us
  starting transfers between devices  69.5 us (36%)
  waiting for transfers between devices  61.7 us (32%)
  blocking collectives  35.6 us (19%)
  Pallas kernels  16.4 us (9%)
  local copies, waits for them, and re-layouts  3.62 us (2%)
  matrix products  2.25 us (1%)
    all_to_all x7, waiting for transfers between devices, exchange(): return lax.all_to_all(pieces, axis, split_axis=0, concat_axis=0, tiled=True)  61.7 us
    all_to_all x7, starting transfers between devices, exchange(): return lax.all_to_all(pieces, axis, split_axis=0, concat_axis=0, tiled=True)  55 us
    all_to_all x2, blocking collectives, exchange(): return lax.all_to_all(pieces, axis, split_axis=0, concat_axis=0, tiled=True)  35.6 us
    pallas_call x13, Pallas kernels, call(): pl.pallas_call(kernel, out_shape=out_shape, scratch_shapes=list(scratch),...  16.4 us
    ppermute x4, starting transfers between devices, step_of(): return lax.ppermute(held, 'dp', [(i, i ^ bit) for i in range(size)])  14.5 us
  transfers between devices with their start and end apart: 11, of which 7 were waited for; matrix products, arithmetic and copies ran while one was open for 3% of the time, Pallas kernels for 5%

commit v1 on v0

--- a/solution.py
+++ b/solution.py
@@ -264,7 +264,7 @@
         specs=[*whole, *blocks, *[pl.BlockSpec(memory_space=pl.ANY) for _ in made]],
         out_specs=blocks,
         aliases={6: 0, 7: 1} if made else None,
-        room=MOST_VMEM - 400 * 2**10,
+        room=(MOST_VMEM - 400 * 2**10) if made else 60 * 1024 * 2**10,
     )
 
 
@@ -349,8 +349,6 @@
                 got,
             )
             x_local = lax.dynamic_slice_in_dim(x_full, me * feats, feats, 1)
-            tied = after(saved[0], (qk,))
-            made = update(0, tied, matrix_state, normalizer_state, ())
         pieces = exchange(qk, "tp")
         gate_pre = (
             jnp.dot(x_full, gate_weight[block_no], preferred_element_type=F32)
@@ -387,6 +385,8 @@
             got,
             scratch=[pltpu.VMEM((owners, seqs, rows), bf16)],
         )
+        if block_no == 0:
+            made = update(0, after(saved[0], summed), matrix_state, normalizer_state, ())
         new_stabs.append(stab_new)
         pieces = exchange(summed, "tp")
     gain = lax.dynamic_slice_in_dim(norm_gain[1:], me * feats, feats, 1)

time: 192 us -> 192 us (level)
  no operation moved by 1% of the time
where the time goes in v1:
time: 192 us; the launch traced here: 191 us
  starting transfers between devices  69.5 us (36%)
  waiting for transfers between devices  61.7 us (32%)
  blocking collectives  35.6 us (19%)
  Pallas kernels  16.4 us (9%)
  local copies, waits for them, and re-layouts  3.62 us (2%)
  matrix products  2.25 us (1%)
    all_to_all x7, waiting for transfers between devices, exchange(): return lax.all_to_all(pieces, axis, split_axis=0, concat_axis=0, tiled=True)  61.7 us
    all_to_all x7, starting transfers between devices, exchange(): return lax.all_to_all(pieces, axis, split_axis=0, concat_axis=0, tiled=True)  55 us
    all_to_all x2, blocking collectives, exchange(): return lax.all_to_all(pieces, axis, split_axis=0, concat_axis=0, tiled=True)  35.6 us
    pallas_call x13, Pallas kernels, call(): pl.pallas_call(kernel, out_shape=out_shape, scratch_shapes=list(scratch),...  16.4 us
    ppermute x4, starting transfers between devices, step_of(): return lax.ppermute(held, 'dp', [(i, i ^ bit) for i in range(size)])  14.5 us
  transfers between devices with their start and end apart: 11, of which 7 were waited for; matrix products, arithmetic and copies ran while one was open for 3% of the time, Pallas kernels for 5%

profile of v1, /device:TPU:2, one launch (start us, length us, event | category | flops | bytes accessed | tf_op | source)
XLA Modules:
  0.0 191.1 jit_solution(7796109135231615091)
XLA Ops:
  2.0 23.4 %all-to-all-start = ((bf16[64,8,128]{2,1,0:T(8,128)(2,1)}), bf16[64,8,128]{2,1,0:T(8,128)(2,1)S(1)}, u32[]{:S(2)}, u32[]{:S(2)}) async-start(bf16[64,8,128]{2,1,0:T(8,128)(2,1)} %shard_map.147), calls=%async_computation | async-start | bytes 262144 | tf_op jit(solution)/shard_map/all_to_all | solution.py:19
  25.4 1.7 shard_map.149
  27.1 6.6 %collective-permute-start = (bf16[1,320,256]{2,1,0:T(8,128)(2,1)}, bf16[1,320,256]{2,1,0:T(8,128)(2,1)S(1)}, u32[]{:S(2)}, u32[]{:S(2)}) collective-permute-start(bf16[1,320,256]{2,1,0:T(8,128)(2,1)} %get-tuple-element.40), channel_id=1, source_target_pairs={{0,8},{1,9},{2,10},{3,11},{4,12},{5,13},{6,14},{7,15},{8,0},{9,1},... | collective-permute-start | bytes 491528 | tf_op jit(solution)/shard_map/ppermute | solution.py:28
  33.8 4.3 %all-to-all-done.pieces_ref = bf16[64,8,128]{2,1,0:T(8,128)(2,1)S(1)} async-done(((bf16[64,8,128]{2,1,0:T(8,128)(2,1)}), bf16[64,8,128]{2,1,0:T(8,128)(2,1)S(1)}, u32[]{:S(2)}, u32[]{:S(2)}) %all-to-all-start) | async-done | bytes 131104 | tf_op jit(solution)/shard_map/all_to_all | solution.py:19
  38.1 0.7 shard_map.148
  38.8 7.3 %all-to-all-start.1 = ((bf16[16,8,256]{2,1,0:T(8,128)(2,1)}), bf16[16,8,256]{2,1,0:T(8,128)(2,1)S(1)}, u32[]{:S(2)}, u32[]{:S(2)}) async-start(bf16[16,8,256]{2,1,0:T(8,128)(2,1)} %get-tuple-element.31), calls=%async_computation.1 | async-start | bytes 131072 | tf_op jit(solution)/shard_map/all_to_all | solution.py:19
  46.1 1.2 fusion.10
  48.9 3.8 %all-to-all-done.1.x_ref = bf16[16,8,256]{2,1,0:T(8,128)(2,1)S(1)} async-done(((bf16[16,8,256]{2,1,0:T(8,128)(2,1)}), bf16[16,8,256]{2,1,0:T(8,128)(2,1)S(1)}, u32[]{:S(2)}, u32[]{:S(2)}) %all-to-all-start.1) | async-done | bytes 65568 | tf_op jit(solution)/shard_map/all_to_all | solution.py:19
  52.9 2.7 %collective-permute-start.1 = (bf16[2,320,256]{2,1,0:T(8,128)(2,1)S(1)}, bf16[2,320,256]{2,1,0:T(8,128)(2,1)S(1)}, u32[]{:S(2)}, u32[]{:S(2)}) collective-permute-start(bf16[2,320,256]{2,1,0:T(8,128)(2,1)S(1)} %pad_maximum_fusion.2), channel_id=1, source_target_pairs={{0,4},{1,5},{2,6},{3,7},{4,0},{5,1},{6,2},{7,3},{8,12},{9,13},{10,... | collective-permute-start | bytes 983048 | tf_op jit(solution)/shard_map/ppermute | solution.py:28
  55.6 18.3 %all_to_all.45.parts_ref = bf16[16,8,192]{2,1,0:T(8,128)(2,1)S(1)} all-to-all(bf16[16,8,192]{2,1,0:T(8,128)(2,1)S(1)} %shard_map.150), channel_id=1, replica_groups=mesh['tp'=64,'dp'=16] {'dp'}, dimensions={0} | all-to-all | bytes 98304 | tf_op jit(solution)/shard_map/all_to_all | solution.py:19
  74.7 3.3 %collective-permute-start.2 = (bf16[4,320,256]{2,1,0:T(8,128)(2,1)S(1)}, bf16[4,320,256]{2,1,0:T(8,128)(2,1)S(1)}, u32[]{:S(2)}, u32[]{:S(2)}) collective-permute-start(bf16[4,320,256]{2,1,0:T(8,128)(2,1)S(1)} %pad_maximum_fusion.1), channel_id=1, source_target_pairs={{0,2},{1,3},{2,0},{3,1},{4,6},{5,7},{6,4},{7,5},{8,10},{9,11},{10,... | collective-permute-start | bytes 1966088 | tf_op jit(solution)/shard_map/ppermute | solution.py:28
  78.0 5.8 %all-to-all-start.3 = ((bf16[64,8,128]{2,1,0:T(8,128)(2,1)}), bf16[64,8,128]{2,1,0:T(8,128)(2,1)S(1)}, u32[]{:S(2)}, u32[]{:S(2)}) async-start(bf16[64,8,128]{2,1,0:T(8,128)(2,1)} %get-tuple-element.36), calls=%async_computation.3 | async-start | bytes 262144 | tf_op jit(solution)/shard_map/all_to_all | solution.py:19
  83.8 1.1 convolution_add_fusion.1
  85.0 11.5 %all-to-all-done.3.pieces_ref.refs_0_ = bf16[64,8,128]{2,1,0:T(8,128)(2,1)S(1)} async-done(((bf16[64,8,128]{2,1,0:T(8,128)(2,1)}), bf16[64,8,128]{2,1,0:T(8,128)(2,1)S(1)}, u32[]{:S(2)}, u32[]{:S(2)}) %all-to-all-start.3) | async-done | bytes 131104 | tf_op jit(solution)/shard_map/all_to_all | solution.py:19
  97.2 1.9 collective-permute-start.3
  99.1 17.3 %all_to_all.46.pieces_ref = bf16[64,8,128]{2,1,0:T(8,128)(2,1)S(1)} all-to-all(bf16[64,8,128]{2,1,0:T(8,128)(2,1)S(1)} %shard_map.152), channel_id=1, replica_groups=mesh['tp'=64,'dp'=16] {'tp'}, dimensions={0} | all-to-all | bytes 262144 | tf_op jit(solution)/shard_map/all_to_all | solution.py:19
  116.4 1.0 shard_map.153
  117.4 4.6 %all-to-all-start.5 = ((bf16[64,8,128]{2,1,0:T(8,128)(2,1)}), bf16[64,8,128]{2,1,0:T(8,128)(2,1)S(1)}, u32[]{:S(2)}, u32[]{:S(2)}) async-start(bf16[64,8,128]{2,1,0:T(8,128)(2,1)} %shard_map.153), calls=%async_computation.5 | async-start | bytes 262144 | tf_op jit(solution)/shard_map/all_to_all | solution.py:19
  122.0 12.7 %all-to-all-done.5.pieces_ref = bf16[64,8,128]{2,1,0:T(8,128)(2,1)S(1)} async-done(((bf16[64,8,128]{2,1,0:T(8,128)(2,1)}), bf16[64,8,128]{2,1,0:T(8,128)(2,1)S(1)}, u32[]{:S(2)}, u32[]{:S(2)}) %all-to-all-start.5) | async-done | bytes 131104 | tf_op jit(solution)/shard_map/all_to_all | solution.py:19
  134.8 1.5 shard_map.154
  136.2 4.6 %all-to-all-start.6 = ((bf16[64,8,128]{2,1,0:T(8,128)(2,1)}), bf16[64,8,128]{2,1,0:T(8,128)(2,1)S(1)}, u32[]{:S(2)}, u32[]{:S(2)}) async-start(bf16[64,8,128]{2,1,0:T(8,128)(2,1)} %get-tuple-element.43), calls=%async_computation.6 | async-start | bytes 262144 | tf_op jit(solution)/shard_map/all_to_all | solution.py:19
  140.8 1.1 convolution_add_fusion
  142.1 11.5 %all-to-all-done.6.pieces_ref.refs_0_ = bf16[64,8,128]{2,1,0:T(8,128)(2,1)S(1)} async-done(((bf16[64,8,128]{2,1,0:T(8,128)(2,1)}), bf16[64,8,128]{2,1,0:T(8,128)(2,1)S(1)}, u32[]{:S(2)}, u32[]{:S(2)}) %all-to-all-start.6) | async-done | bytes 131104 | tf_op jit(solution)/shard_map/all_to_all | solution.py:19
  153.6 1.1 shard_map.155
  154.6 4.6 %all-to-all-start.7 = ((bf16[64,8,128]{2,1,0:T(8,128)(2,1)}), bf16[64,8,128]{2,1,0:T(8,128)(2,1)S(1)}, u32[]{:S(2)}, u32[]{:S(2)}) async-start(bf16[64,8,128]{2,1,0:T(8,128)(2,1)} %shard_map.155), calls=%async_computation.7 | async-start | bytes 262144 | tf_op jit(solution)/shard_map/all_to_all | solution.py:19
  159.3 12.6 %all-to-all-done.7.pieces_ref = bf16[64,8,128]{2,1,0:T(8,128)(2,1)S(1)} async-done(((bf16[64,8,128]{2,1,0:T(8,128)(2,1)}), bf16[64,8,128]{2,1,0:T(8,128)(2,1)S(1)}, u32[]{:S(2)}, u32[]{:S(2)}) %all-to-all-start.7) | async-done | bytes 131104 | tf_op jit(solution)/shard_map/all_to_all | solution.py:19
  171.9 1.0 shard_map.156
  172.9 4.6 %all-to-all-start.8 = ((bf16[64,8,128]{2,1,0:T(8,128)(2,1)}), bf16[64,8,128]{2,1,0:T(8,128)(2,1)S(1)}, u32[]{:S(2)}, u32[]{:S(2)}) async-start(bf16[64,8,128]{2,1,0:T(8,128)(2,1)} %shard_map.156), calls=%async_computation.8 | async-start | bytes 262144 | tf_op jit(solution)/shard_map/all_to_all | solution.py:19
  177.6 3.3 %shard_map.158 = (f32[2,8,3,16,192]{4,3,2,1,0:T(8,128)}, f32[2,8,16,192]{3,2,1,0:T(8,128)}) custom-call(bf16[64,8,128]{2,1,0:T(8,128)(2,1)} %copy-done, bf16[8,96]{1,0:T(8,128)(2,1)} %copy-done.9, f32[8,16]{1,0:T(8,128)} %copy-done.4, f32[8,16]{1,0:T(8,128)} %copy-done.3, f32[2,8,3,16,192]{4,3,2,1,0:T(8,128)} %refs_4_.3, f32[2,8,16,192]{3,2,1,0:T(8,128)} %refs_5_.3), custom_call_target="tpu_custom_call" | custom-call | flops 1000000 | bytes 920064 | tf_op jit(solution)/shard_map/pallas_call | solution.py:83
  181.6 3.3 %shard_map.159 = (f32[2,8,3,16,192]{4,3,2,1,0:T(8,128)}, f32[2,8,16,192]{3,2,1,0:T(8,128)}) custom-call(bf16[64,8,128]{2,1,0:T(8,128)(2,1)} %copy-done.1, bf16[8,96]{1,0:T(8,128)(2,1)} %copy-done.10, f32[8,16]{1,0:T(8,128)} %copy-done.6, f32[8,16]{1,0:T(8,128)} %copy-done.5, ...), custom_call_target="tpu_custom_call", output_to_operand_aliasing={{0}: (6, {}), {1}: (7, {})} | custom-call | flops 1000000 | bytes 1706496 | tf_op jit(solution)/shard_map/pallas_call | solution.py:83
  184.9 5.4 %all-to-all-done.8.pieces_ref = bf16[64,8,128]{2,1,0:T(8,128)(2,1)S(1)} async-done(((bf16[64,8,128]{2,1,0:T(8,128)(2,1)}), bf16[64,8,128]{2,1,0:T(8,128)(2,1)S(1)}, u32[]{:S(2)}, u32[]{:S(2)}) %all-to-all-start.8) | async-done | bytes 131104 | tf_op jit(solution)/shard_map/all_to_all | solution.py:19
  190.3 0.9 shard_map.157
  (59 shorter events, 5.4 us)
Async XLA Ops:
  0.6 0.7 copy-start.7
  2.0 36.1 %all-to-all-start = ((bf16[64,8,128]{2,1,0:T(8,128)(2,1)}), bf16[64,8,128]{2,1,0:T(8,128)(2,1)S(1)}, u32[]{:S(2)}, u32[]{:S(2)}) async-start(bf16[64,8,128]{2,1,0:T(8,128)(2,1)} %shard_map.147), calls=%async_computation | async-start | bytes 262144 | tf_op jit(solution)/shard_map/all_to_all | solution.py:19
  27.1 20.2 %copy-start.11 = (f32[2,8,16,192]{3,2,1,0:T(8,128)S(1)}, f32[2,8,16,192]{3,2,1,0:T(8,128)}, u32[]{:S(2)}) copy-start(f32[2,8,16,192]{3,2,1,0:T(8,128)} %refs_5_.3) | copy-start | bytes 589828
  27.1 25.7 %collective-permute-start = (bf16[1,320,256]{2,1,0:T(8,128)(2,1)}, bf16[1,320,256]{2,1,0:T(8,128)(2,1)S(1)}, u32[]{:S(2)}, u32[]{:S(2)}) collective-permute-start(bf16[1,320,256]{2,1,0:T(8,128)(2,1)} %get-tuple-element.40), channel_id=1, source_target_pairs={{0,8},{1,9},{2,10},{3,11},{4,12},{5,13},{6,14},{7,15},{8,0},{9,1},... | collective-permute-start | bytes 491528 | tf_op jit(solution)/shard_map/ppermute | solution.py:28
  38.8 13.8 %all-to-all-start.1 = ((bf16[16,8,256]{2,1,0:T(8,128)(2,1)}), bf16[16,8,256]{2,1,0:T(8,128)(2,1)S(1)}, u32[]{:S(2)}, u32[]{:S(2)}) async-start(bf16[16,8,256]{2,1,0:T(8,128)(2,1)} %get-tuple-element.31), calls=%async_computation.1 | async-start | bytes 131072 | tf_op jit(solution)/shard_map/all_to_all | solution.py:19
  48.1 4.6 %copy-start.2 = (bf16[192,256]{1,0:T(8,128)(2,1)S(1)}, bf16[192,256]{1,0:T(8,128)(2,1)}, u32[]{:S(2)}) copy-start(bf16[192,256]{1,0:T(8,128)(2,1)} %get-tuple-element.32.weight_ref) | copy-start | bytes 294916
  48.1 4.8 %copy-start.12 = (bf16[1,320,256]{2,1,0:T(8,128)(2,1)S(1)}, bf16[1,320,256]{2,1,0:T(8,128)(2,1)}, u32[]{:S(2)}) copy-start(bf16[1,320,256]{2,1,0:T(8,128)(2,1)} %get-tuple-element.40) | copy-start | bytes 491524
  48.9 29.1 %copy-start.15 = (f32[2,32]{1,0:T(2,128)S(1)}, f32[2,32]{1,0:T(2,128)}, u32[]{:S(2)}) copy-start(f32[2,32]{1,0:T(2,128)} %param.18) | copy-start | bytes 772
  52.8 32.1 %copy-start.14 = (f32[2,8,16]{2,1,0:T(8,128)S(1)}, f32[2,8,16]{2,1,0:T(8,128)}, u32[]{:S(2)}) copy-start(f32[2,8,16]{2,1,0:T(8,128)} %param.23) | copy-start | bytes 3076
  52.9 21.7 %collective-permute-start.1 = (bf16[2,320,256]{2,1,0:T(8,128)(2,1)S(1)}, bf16[2,320,256]{2,1,0:T(8,128)(2,1)S(1)}, u32[]{:S(2)}, u32[]{:S(2)}) collective-permute-start(bf16[2,320,256]{2,1,0:T(8,128)(2,1)S(1)} %pad_maximum_fusion.2), channel_id=1, source_target_pairs={{0,4},{1,5},{2,6},{3,7},{4,0},{5,1},{6,2},{7,3},{8,12},{9,13},{10,... | collective-permute-start | bytes 983048 | tf_op jit(solution)/shard_map/ppermute | solution.py:28
  74.6 22.3 %copy-start.9 = (bf16[8,96]{1,0:T(8,128)(2,1)}, bf16[8,96]{1,0:T(8,128)(2,1)S(1)}, u32[]{:S(2)}) copy-start(bf16[8,96]{1,0:T(8,128)(2,1)S(1)} %get-tuple-element.51.vo_ref.refs_1_) | copy-start | bytes 4612
  74.7 22.3 %collective-permute-start.2 = (bf16[4,320,256]{2,1,0:T(8,128)(2,1)S(1)}, bf16[4,320,256]{2,1,0:T(8,128)(2,1)S(1)}, u32[]{:S(2)}, u32[]{:S(2)}) collective-permute-start(bf16[4,320,256]{2,1,0:T(8,128)(2,1)S(1)} %pad_maximum_fusion.1), channel_id=1, source_target_pairs={{0,2},{1,3},{2,0},{3,1},{4,6},{5,7},{6,4},{7,5},{8,10},{9,11},{10,... | collective-permute-start | bytes 1966088 | tf_op jit(solution)/shard_map/ppermute | solution.py:28
  78.0 18.5 %all-to-all-start.3 = ((bf16[64,8,128]{2,1,0:T(8,128)(2,1)}), bf16[64,8,128]{2,1,0:T(8,128)(2,1)S(1)}, u32[]{:S(2)}, u32[]{:S(2)}) async-start(bf16[64,8,128]{2,1,0:T(8,128)(2,1)} %get-tuple-element.36), calls=%async_computation.3 | async-start | bytes 262144 | tf_op jit(solution)/shard_map/all_to_all | solution.py:19
  85.0 12.0 %copy-start.3 = (f32[8,16]{1,0:T(8,128)}, f32[8,16]{1,0:T(8,128)S(1)}, u32[]{:S(2)}) copy-start(f32[8,16]{1,0:T(8,128)S(1)} %get-tuple-element.53.admit_ref.refs_3_) | copy-start | bytes 1540
  85.0 12.0 %copy-start.4 = (f32[8,16]{1,0:T(8,128)}, f32[8,16]{1,0:T(8,128)S(1)}, u32[]{:S(2)}) copy-start(f32[8,16]{1,0:T(8,128)S(1)} %get-tuple-element.52.retain_ref.refs_2_) | copy-start | bytes 1540
  96.5 0.7 copy-start
  96.9 19.4 %copy-start.8 = (bf16[8,64]{1,0:T(8,128)(2,1)S(1)}, bf16[8,64]{1,0:T(8,128)(2,1)}, u32[]{:S(2)}) copy-start(bf16[8,64]{1,0:T(8,128)(2,1)} %x_ref.3) | copy-start | bytes 3076
  97.2 19.2 %collective-permute-start.3 = (bf16[8,320,256]{2,1,0:T(8,128)(2,1)S(1)}, bf16[8,320,256]{2,1,0:T(8,128)(2,1)S(1)}, u32[]{:S(2)}, u32[]{:S(2)}) collective-permute-start(bf16[8,320,256]{2,1,0:T(8,128)(2,1)S(1)} %pad_maximum_fusion.held_ref), channel_id=1, source_target_pairs={{0,1},{1,0},{2,3},{3,2},{4,5},{5,4},{6,7},{7,6},{8,9},{9,8},{10,11... | collective-permute-start | bytes 3932168 | tf_op jit(solution)/shard_map/ppermute | solution.py:28
  116.4 5.6 %copy-start.13 = (f32[2,4096]{1,0:T(2,128)S(1)}, f32[2,4096]{1,0:T(2,128)}, u32[]{:S(2)}) copy-start(f32[2,4096]{1,0:T(2,128)} %param.20) | copy-start | bytes 98308
  117.4 17.4 %all-to-all-start.5 = ((bf16[64,8,128]{2,1,0:T(8,128)(2,1)}), bf16[64,8,128]{2,1,0:T(8,128)(2,1)S(1)}, u32[]{:S(2)}, u32[]{:S(2)}) async-start(bf16[64,8,128]{2,1,0:T(8,128)(2,1)} %shard_map.153), calls=%async_computation.5 | async-start | bytes 262144 | tf_op jit(solution)/shard_map/all_to_all | solution.py:19
  136.2 36.7 %copy-start.10 = (bf16[8,96]{1,0:T(8,128)(2,1)}, bf16[8,96]{1,0:T(8,128)(2,1)S(1)}, u32[]{:S(2)}) copy-start(bf16[8,96]{1,0:T(8,128)(2,1)S(1)} %get-tuple-element.47.vo_ref.refs_1_) | copy-start | bytes 4612
  136.2 17.4 %all-to-all-start.6 = ((bf16[64,8,128]{2,1,0:T(8,128)(2,1)}), bf16[64,8,128]{2,1,0:T(8,128)(2,1)S(1)}, u32[]{:S(2)}, u32[]{:S(2)}) async-start(bf16[64,8,128]{2,1,0:T(8,128)(2,1)} %get-tuple-element.43), calls=%async_computation.6 | async-start | bytes 262144 | tf_op jit(solution)/shard_map/all_to_all | solution.py:19
  142.1 30.9 %copy-start.5 = (f32[8,16]{1,0:T(8,128)}, f32[8,16]{1,0:T(8,128)S(1)}, u32[]{:S(2)}) copy-start(f32[8,16]{1,0:T(8,128)S(1)} %get-tuple-element.49.admit_ref.refs_3_) | copy-start | bytes 1540
  142.1 30.9 %copy-start.6 = (f32[8,16]{1,0:T(8,128)}, f32[8,16]{1,0:T(8,128)S(1)}, u32[]{:S(2)}) copy-start(f32[8,16]{1,0:T(8,128)S(1)} %get-tuple-element.48.retain_ref.refs_2_) | copy-start | bytes 1540
  153.6 19.4 %copy-start.1 = (bf16[64,8,128]{2,1,0:T(8,128)(2,1)}, bf16[64,8,128]{2,1,0:T(8,128)(2,1)S(1)}, u32[]{:S(2)}) copy-start(bf16[64,8,128]{2,1,0:T(8,128)(2,1)S(1)} %all-to-all-done.6.pieces_ref.refs_0_) | copy-start | bytes 393220
  154.6 17.3 %all-to-all-start.7 = ((bf16[64,8,128]{2,1,0:T(8,128)(2,1)}), bf16[64,8,128]{2,1,0:T(8,128)(2,1)S(1)}, u32[]{:S(2)}, u32[]{:S(2)}) async-start(bf16[64,8,128]{2,1,0:T(8,128)(2,1)} %shard_map.155), calls=%async_computation.7 | async-start | bytes 262144 | tf_op jit(solution)/shard_map/all_to_all | solution.py:19
  172.9 17.3 %all-to-all-start.8 = ((bf16[64,8,128]{2,1,0:T(8,128)(2,1)}), bf16[64,8,128]{2,1,0:T(8,128)(2,1)S(1)}, u32[]{:S(2)}, u32[]{:S(2)}) async-start(bf16[64,8,128]{2,1,0:T(8,128)(2,1)} %shard_map.156), calls=%async_computation.8 | async-start | bytes 262144 | tf_op jit(solution)/shard_map/all_to_all | solution.py:19

commit v2 on v1

--- a/solution.py
+++ b/solution.py
@@ -121,8 +121,11 @@
         at += size
 
 
-def copies_kernel(x_ref, out_ref):
-    spread(out_ref, x_ref[...].astype(F32))
+def copies_kernel(x_ref, out_ref, here_ref, sem):
+    fetch = pltpu.make_async_copy(x_ref, here_ref, sem)
+    fetch.start()
+    fetch.wait()
+    spread(out_ref, here_ref[...].astype(F32))
 
 
 def whole_kernel(pieces_ref, x_ref, cut_ref):
@@ -316,7 +319,17 @@
         return jnp.moveaxis(x, 0, -2).reshape(*x.shape[1:-3], peers // 2, seqs, pair_cols)
 
     whole_x = jax.ShapeDtypeStruct((seqs, peers * feats), bf16)
-    pieces = exchange(call(copies_kernel, copies, stream), "tp")
+    pieces = exchange(
+        call(
+            copies_kernel,
+            copies,
+            stream,
+            specs=[held_in],
+            scratch=[pltpu.VMEM(stream.shape, bf16), pltpu.SemaphoreType.DMA],
+            room=MOST_VMEM,
+        ),
+        "tp",
+    )
     got = step_of(chain, 8)
     x_local = stream
     x_full, cut = call(

time: 192 us -> 192 us (level)
  no operation moved by 1% of the time
where the time goes in v2:
time: 192 us; the launch traced here: 191 us
  starting transfers between devices  69.5 us (36%)
  waiting for transfers between devices  61.7 us (32%)
  blocking collectives  35.6 us (19%)
  Pallas kernels  17.1 us (9%)
  local copies, waits for them, and re-layouts  2.94 us (2%)
  matrix products  2.25 us (1%)
    all_to_all x7, waiting for transfers between devices, exchange(): return lax.all_to_all(pieces, axis, split_axis=0, concat_axis=0, tiled=True)  61.7 us
    all_to_all x7, starting transfers between devices, exchange(): return lax.all_to_all(pieces, axis, split_axis=0, concat_axis=0, tiled=True)  55 us
    all_to_all x2, blocking collectives, exchange(): return lax.all_to_all(pieces, axis, split_axis=0, concat_axis=0, tiled=True)  35.6 us
    pallas_call x13, Pallas kernels, call(): pl.pallas_call(kernel, out_shape=out_shape, scratch_shapes=list(scratch),...  17.1 us
    ppermute x4, starting transfers between devices, step_of(): return lax.ppermute(held, 'dp', [(i, i ^ bit) for i in range(size)])  14.5 us
  transfers between devices with their start and end apart: 11, of which 7 were waited for; matrix products, arithmetic and copies ran while one was open for 3% of the time, Pallas kernels for 5%

profile of v2, /device:TPU:2, one launch (start us, length us, event | category | flops | bytes accessed | tf_op | source)
XLA Modules:
  0.0 191.2 jit_solution(10745586325338562731)
XLA Ops:
  0.6 1.4 shard_map.147
  2.0 23.4 %all-to-all-start = ((bf16[64,8,128]{2,1,0:T(8,128)(2,1)}), bf16[64,8,128]{2,1,0:T(8,128)(2,1)S(1)}, u32[]{:S(2)}, u32[]{:S(2)}) async-start(bf16[64,8,128]{2,1,0:T(8,128)(2,1)} %shard_map.147), calls=%async_computation | async-start | bytes 262144 | tf_op jit(solution)/shard_map/all_to_all | solution.py:19
  25.4 1.7 shard_map.149
  27.1 6.6 %collective-permute-start = (bf16[1,320,256]{2,1,0:T(8,128)(2,1)}, bf16[1,320,256]{2,1,0:T(8,128)(2,1)S(1)}, u32[]{:S(2)}, u32[]{:S(2)}) collective-permute-start(bf16[1,320,256]{2,1,0:T(8,128)(2,1)} %get-tuple-element.40), channel_id=1, source_target_pairs={{0,8},{1,9},{2,10},{3,11},{4,12},{5,13},{6,14},{7,15},{8,0},{9,1},... | collective-permute-start | bytes 491528 | tf_op jit(solution)/shard_map/ppermute | solution.py:28
  33.8 4.3 %all-to-all-done.pieces_ref = bf16[64,8,128]{2,1,0:T(8,128)(2,1)S(1)} async-done(((bf16[64,8,128]{2,1,0:T(8,128)(2,1)}), bf16[64,8,128]{2,1,0:T(8,128)(2,1)S(1)}, u32[]{:S(2)}, u32[]{:S(2)}) %all-to-all-start) | async-done | bytes 131104 | tf_op jit(solution)/shard_map/all_to_all | solution.py:19
  38.9 7.3 %all-to-all-start.1 = ((bf16[16,8,256]{2,1,0:T(8,128)(2,1)}), bf16[16,8,256]{2,1,0:T(8,128)(2,1)S(1)}, u32[]{:S(2)}, u32[]{:S(2)}) async-start(bf16[16,8,256]{2,1,0:T(8,128)(2,1)} %get-tuple-element.31), calls=%async_computation.1 | async-start | bytes 131072 | tf_op jit(solution)/shard_map/all_to_all | solution.py:19
  46.2 1.2 fusion.10
  48.9 3.8 %all-to-all-done.1.x_ref = bf16[16,8,256]{2,1,0:T(8,128)(2,1)S(1)} async-done(((bf16[16,8,256]{2,1,0:T(8,128)(2,1)}), bf16[16,8,256]{2,1,0:T(8,128)(2,1)S(1)}, u32[]{:S(2)}, u32[]{:S(2)}) %all-to-all-start.1) | async-done | bytes 65568 | tf_op jit(solution)/shard_map/all_to_all | solution.py:19
  52.9 2.7 %collective-permute-start.1 = (bf16[2,320,256]{2,1,0:T(8,128)(2,1)S(1)}, bf16[2,320,256]{2,1,0:T(8,128)(2,1)S(1)}, u32[]{:S(2)}, u32[]{:S(2)}) collective-permute-start(bf16[2,320,256]{2,1,0:T(8,128)(2,1)S(1)} %pad_maximum_fusion.2), channel_id=1, source_target_pairs={{0,4},{1,5},{2,6},{3,7},{4,0},{5,1},{6,2},{7,3},{8,12},{9,13},{10,... | collective-permute-start | bytes 983048 | tf_op jit(solution)/shard_map/ppermute | solution.py:28
  55.7 18.3 %all_to_all.45.parts_ref = bf16[16,8,192]{2,1,0:T(8,128)(2,1)S(1)} all-to-all(bf16[16,8,192]{2,1,0:T(8,128)(2,1)S(1)} %shard_map.150), channel_id=1, replica_groups=mesh['tp'=64,'dp'=16] {'dp'}, dimensions={0} | all-to-all | bytes 98304 | tf_op jit(solution)/shard_map/all_to_all | solution.py:19
  74.7 3.3 %collective-permute-start.2 = (bf16[4,320,256]{2,1,0:T(8,128)(2,1)S(1)}, bf16[4,320,256]{2,1,0:T(8,128)(2,1)S(1)}, u32[]{:S(2)}, u32[]{:S(2)}) collective-permute-start(bf16[4,320,256]{2,1,0:T(8,128)(2,1)S(1)} %pad_maximum_fusion.1), channel_id=1, source_target_pairs={{0,2},{1,3},{2,0},{3,1},{4,6},{5,7},{6,4},{7,5},{8,10},{9,11},{10,... | collective-permute-start | bytes 1966088 | tf_op jit(solution)/shard_map/ppermute | solution.py:28
  78.0 5.8 %all-to-all-start.3 = ((bf16[64,8,128]{2,1,0:T(8,128)(2,1)}), bf16[64,8,128]{2,1,0:T(8,128)(2,1)S(1)}, u32[]{:S(2)}, u32[]{:S(2)}) async-start(bf16[64,8,128]{2,1,0:T(8,128)(2,1)} %get-tuple-element.36), calls=%async_computation.3 | async-start | bytes 262144 | tf_op jit(solution)/shard_map/all_to_all | solution.py:19
  83.8 1.1 convolution_add_fusion.1
  85.1 11.5 %all-to-all-done.3.pieces_ref.refs_0_ = bf16[64,8,128]{2,1,0:T(8,128)(2,1)S(1)} async-done(((bf16[64,8,128]{2,1,0:T(8,128)(2,1)}), bf16[64,8,128]{2,1,0:T(8,128)(2,1)S(1)}, u32[]{:S(2)}, u32[]{:S(2)}) %all-to-all-start.3) | async-done | bytes 131104 | tf_op jit(solution)/shard_map/all_to_all | solution.py:19
  97.2 1.9 collective-permute-start.3
  99.1 17.3 %all_to_all.46.pieces_ref = bf16[64,8,128]{2,1,0:T(8,128)(2,1)S(1)} all-to-all(bf16[64,8,128]{2,1,0:T(8,128)(2,1)S(1)} %shard_map.152), channel_id=1, replica_groups=mesh['tp'=64,'dp'=16] {'tp'}, dimensions={0} | all-to-all | bytes 262144 | tf_op jit(solution)/shard_map/all_to_all | solution.py:19
  116.4 1.0 shard_map.153
  117.4 4.6 %all-to-all-start.5 = ((bf16[64,8,128]{2,1,0:T(8,128)(2,1)}), bf16[64,8,128]{2,1,0:T(8,128)(2,1)S(1)}, u32[]{:S(2)}, u32[]{:S(2)}) async-start(bf16[64,8,128]{2,1,0:T(8,128)(2,1)} %shard_map.153), calls=%async_computation.5 | async-start | bytes 262144 | tf_op jit(solution)/shard_map/all_to_all | solution.py:19
  122.1 12.7 %all-to-all-done.5.pieces_ref = bf16[64,8,128]{2,1,0:T(8,128)(2,1)S(1)} async-done(((bf16[64,8,128]{2,1,0:T(8,128)(2,1)}), bf16[64,8,128]{2,1,0:T(8,128)(2,1)S(1)}, u32[]{:S(2)}, u32[]{:S(2)}) %all-to-all-start.5) | async-done | bytes 131104 | tf_op jit(solution)/shard_map/all_to_all | solution.py:19
  134.8 1.5 shard_map.154
  136.2 4.6 %all-to-all-start.6 = ((bf16[64,8,128]{2,1,0:T(8,128)(2,1)}), bf16[64,8,128]{2,1,0:T(8,128)(2,1)S(1)}, u32[]{:S(2)}, u32[]{:S(2)}) async-start(bf16[64,8,128]{2,1,0:T(8,128)(2,1)} %get-tuple-element.43), calls=%async_computation.6 | async-start | bytes 262144 | tf_op jit(solution)/shard_map/all_to_all | solution.py:19
  140.9 1.1 convolution_add_fusion
  142.1 11.5 %all-to-all-done.6.pieces_ref.refs_0_ = bf16[64,8,128]{2,1,0:T(8,128)(2,1)S(1)} async-done(((bf16[64,8,128]{2,1,0:T(8,128)(2,1)}), bf16[64,8,128]{2,1,0:T(8,128)(2,1)S(1)}, u32[]{:S(2)}, u32[]{:S(2)}) %all-to-all-start.6) | async-done | bytes 131104 | tf_op jit(solution)/shard_map/all_to_all | solution.py:19
  153.6 1.1 shard_map.155
  154.7 4.6 %all-to-all-start.7 = ((bf16[64,8,128]{2,1,0:T(8,128)(2,1)}), bf16[64,8,128]{2,1,0:T(8,128)(2,1)S(1)}, u32[]{:S(2)}, u32[]{:S(2)}) async-start(bf16[64,8,128]{2,1,0:T(8,128)(2,1)} %shard_map.155), calls=%async_computation.7 | async-start | bytes 262144 | tf_op jit(solution)/shard_map/all_to_all | solution.py:19
  159.4 12.6 %all-to-all-done.7.pieces_ref = bf16[64,8,128]{2,1,0:T(8,128)(2,1)S(1)} async-done(((bf16[64,8,128]{2,1,0:T(8,128)(2,1)}), bf16[64,8,128]{2,1,0:T(8,128)(2,1)S(1)}, u32[]{:S(2)}, u32[]{:S(2)}) %all-to-all-start.7) | async-done | bytes 131104 | tf_op jit(solution)/shard_map/all_to_all | solution.py:19
  172.0 1.0 shard_map.156
  173.0 4.6 %all-to-all-start.8 = ((bf16[64,8,128]{2,1,0:T(8,128)(2,1)}), bf16[64,8,128]{2,1,0:T(8,128)(2,1)S(1)}, u32[]{:S(2)}, u32[]{:S(2)}) async-start(bf16[64,8,128]{2,1,0:T(8,128)(2,1)} %shard_map.156), calls=%async_computation.8 | async-start | bytes 262144 | tf_op jit(solution)/shard_map/all_to_all | solution.py:19
  177.7 3.3 %shard_map.158 = (f32[2,8,3,16,192]{4,3,2,1,0:T(8,128)}, f32[2,8,16,192]{3,2,1,0:T(8,128)}) custom-call(bf16[64,8,128]{2,1,0:T(8,128)(2,1)} %copy-done, bf16[8,96]{1,0:T(8,128)(2,1)} %copy-done.8, f32[8,16]{1,0:T(8,128)} %copy-done.4, f32[8,16]{1,0:T(8,128)} %copy-done.3, f32[2,8,3,16,192]{4,3,2,1,0:T(8,128)} %refs_4_.3, f32[2,8,16,192]{3,2,1,0:T(8,128)} %refs_5_.3), custom_call_target="tpu_custom_call" | custom-call | flops 1000000 | bytes 920064 | tf_op jit(solution)/shard_map/pallas_call | solution.py:83
  181.6 3.3 %shard_map.159 = (f32[2,8,3,16,192]{4,3,2,1,0:T(8,128)}, f32[2,8,16,192]{3,2,1,0:T(8,128)}) custom-call(bf16[64,8,128]{2,1,0:T(8,128)(2,1)} %copy-done.1, bf16[8,96]{1,0:T(8,128)(2,1)} %copy-done.9, f32[8,16]{1,0:T(8,128)} %copy-done.6, f32[8,16]{1,0:T(8,128)} %copy-done.5, ...), custom_call_target="tpu_custom_call", output_to_operand_aliasing={{0}: (6, {}), {1}: (7, {})} | custom-call | flops 1000000 | bytes 1706496 | tf_op jit(solution)/shard_map/pallas_call | solution.py:83
  184.9 5.4 %all-to-all-done.8.pieces_ref = bf16[64,8,128]{2,1,0:T(8,128)(2,1)S(1)} async-done(((bf16[64,8,128]{2,1,0:T(8,128)(2,1)}), bf16[64,8,128]{2,1,0:T(8,128)(2,1)S(1)}, u32[]{:S(2)}, u32[]{:S(2)}) %all-to-all-start.8) | async-done | bytes 131104 | tf_op jit(solution)/shard_map/all_to_all | solution.py:19
  190.3 0.9 shard_map.157
  (57 shorter events, 4.8 us)
Async XLA Ops:
  2.0 36.1 %all-to-all-start = ((bf16[64,8,128]{2,1,0:T(8,128)(2,1)}), bf16[64,8,128]{2,1,0:T(8,128)(2,1)S(1)}, u32[]{:S(2)}, u32[]{:S(2)}) async-start(bf16[64,8,128]{2,1,0:T(8,128)(2,1)} %shard_map.147), calls=%async_computation | async-start | bytes 262144 | tf_op jit(solution)/shard_map/all_to_all | solution.py:19
  27.1 20.2 %copy-start.10 = (f32[2,8,16,192]{3,2,1,0:T(8,128)S(1)}, f32[2,8,16,192]{3,2,1,0:T(8,128)}, u32[]{:S(2)}) copy-start(f32[2,8,16,192]{3,2,1,0:T(8,128)} %refs_5_.3) | copy-start | bytes 589828
  27.1 25.7 %collective-permute-start = (bf16[1,320,256]{2,1,0:T(8,128)(2,1)}, bf16[1,320,256]{2,1,0:T(8,128)(2,1)S(1)}, u32[]{:S(2)}, u32[]{:S(2)}) collective-permute-start(bf16[1,320,256]{2,1,0:T(8,128)(2,1)} %get-tuple-element.40), channel_id=1, source_target_pairs={{0,8},{1,9},{2,10},{3,11},{4,12},{5,13},{6,14},{7,15},{8,0},{9,1},... | collective-permute-start | bytes 491528 | tf_op jit(solution)/shard_map/ppermute | solution.py:28
  38.9 13.8 %all-to-all-start.1 = ((bf16[16,8,256]{2,1,0:T(8,128)(2,1)}), bf16[16,8,256]{2,1,0:T(8,128)(2,1)S(1)}, u32[]{:S(2)}, u32[]{:S(2)}) async-start(bf16[16,8,256]{2,1,0:T(8,128)(2,1)} %get-tuple-element.31), calls=%async_computation.1 | async-start | bytes 131072 | tf_op jit(solution)/shard_map/all_to_all | solution.py:19
  48.1 4.6 %copy-start.2 = (bf16[192,256]{1,0:T(8,128)(2,1)S(1)}, bf16[192,256]{1,0:T(8,128)(2,1)}, u32[]{:S(2)}) copy-start(bf16[192,256]{1,0:T(8,128)(2,1)} %get-tuple-element.32.weight_ref) | copy-start | bytes 294916
  48.1 4.8 %copy-start.11 = (bf16[1,320,256]{2,1,0:T(8,128)(2,1)S(1)}, bf16[1,320,256]{2,1,0:T(8,128)(2,1)}, u32[]{:S(2)}) copy-start(bf16[1,320,256]{2,1,0:T(8,128)(2,1)} %get-tuple-element.40) | copy-start | bytes 491524
  48.9 29.1 %copy-start.14 = (f32[2,32]{1,0:T(2,128)S(1)}, f32[2,32]{1,0:T(2,128)}, u32[]{:S(2)}) copy-start(f32[2,32]{1,0:T(2,128)} %param.18) | copy-start | bytes 772
  52.8 32.1 %copy-start.13 = (f32[2,8,16]{2,1,0:T(8,128)S(1)}, f32[2,8,16]{2,1,0:T(8,128)}, u32[]{:S(2)}) copy-start(f32[2,8,16]{2,1,0:T(8,128)} %param.23) | copy-start | bytes 3076
  52.9 21.7 %collective-permute-start.1 = (bf16[2,320,256]{2,1,0:T(8,128)(2,1)S(1)}, bf16[2,320,256]{2,1,0:T(8,128)(2,1)S(1)}, u32[]{:S(2)}, u32[]{:S(2)}) collective-permute-start(bf16[2,320,256]{2,1,0:T(8,128)(2,1)S(1)} %pad_maximum_fusion.2), channel_id=1, source_target_pairs={{0,4},{1,5},{2,6},{3,7},{4,0},{5,1},{6,2},{7,3},{8,12},{9,13},{10,... | collective-permute-start | bytes 983048 | tf_op jit(solution)/shard_map/ppermute | solution.py:28
  74.6 22.3 %copy-start.8 = (bf16[8,96]{1,0:T(8,128)(2,1)}, bf16[8,96]{1,0:T(8,128)(2,1)S(1)}, u32[]{:S(2)}) copy-start(bf16[8,96]{1,0:T(8,128)(2,1)S(1)} %get-tuple-element.51.vo_ref.refs_1_) | copy-start | bytes 4612
  74.7 22.3 %collective-permute-start.2 = (bf16[4,320,256]{2,1,0:T(8,128)(2,1)S(1)}, bf16[4,320,256]{2,1,0:T(8,128)(2,1)S(1)}, u32[]{:S(2)}, u32[]{:S(2)}) collective-permute-start(bf16[4,320,256]{2,1,0:T(8,128)(2,1)S(1)} %pad_maximum_fusion.1), channel_id=1, source_target_pairs={{0,2},{1,3},{2,0},{3,1},{4,6},{5,7},{6,4},{7,5},{8,10},{9,11},{10,... | collective-permute-start | bytes 1966088 | tf_op jit(solution)/shard_map/ppermute | solution.py:28
  78.0 18.5 %all-to-all-start.3 = ((bf16[64,8,128]{2,1,0:T(8,128)(2,1)}), bf16[64,8,128]{2,1,0:T(8,128)(2,1)S(1)}, u32[]{:S(2)}, u32[]{:S(2)}) async-start(bf16[64,8,128]{2,1,0:T(8,128)(2,1)} %get-tuple-element.36), calls=%async_computation.3 | async-start | bytes 262144 | tf_op jit(solution)/shard_map/all_to_all | solution.py:19
  85.0 12.0 %copy-start.3 = (f32[8,16]{1,0:T(8,128)}, f32[8,16]{1,0:T(8,128)S(1)}, u32[]{:S(2)}) copy-start(f32[8,16]{1,0:T(8,128)S(1)} %get-tuple-element.53.admit_ref.refs_3_) | copy-start | bytes 1540
  85.1 12.0 %copy-start.4 = (f32[8,16]{1,0:T(8,128)}, f32[8,16]{1,0:T(8,128)S(1)}, u32[]{:S(2)}) copy-start(f32[8,16]{1,0:T(8,128)S(1)} %get-tuple-element.52.retain_ref.refs_2_) | copy-start | bytes 1540
  96.5 0.7 copy-start
  96.9 19.4 %copy-start.7 = (bf16[8,64]{1,0:T(8,128)(2,1)S(1)}, bf16[8,64]{1,0:T(8,128)(2,1)}, u32[]{:S(2)}) copy-start(bf16[8,64]{1,0:T(8,128)(2,1)} %x_ref.3) | copy-start | bytes 3076
  97.2 19.2 %collective-permute-start.3 = (bf16[8,320,256]{2,1,0:T(8,128)(2,1)S(1)}, bf16[8,320,256]{2,1,0:T(8,128)(2,1)S(1)}, u32[]{:S(2)}, u32[]{:S(2)}) collective-permute-start(bf16[8,320,256]{2,1,0:T(8,128)(2,1)S(1)} %pad_maximum_fusion.held_ref), channel_id=1, source_target_pairs={{0,1},{1,0},{2,3},{3,2},{4,5},{5,4},{6,7},{7,6},{8,9},{9,8},{10,11... | collective-permute-start | bytes 3932168 | tf_op jit(solution)/shard_map/ppermute | solution.py:28
  116.4 5.6 %copy-start.12 = (f32[2,4096]{1,0:T(2,128)S(1)}, f32[2,4096]{1,0:T(2,128)}, u32[]{:S(2)}) copy-start(f32[2,4096]{1,0:T(2,128)} %param.20) | copy-start | bytes 98308
  117.4 17.4 %all-to-all-start.5 = ((bf16[64,8,128]{2,1,0:T(8,128)(2,1)}), bf16[64,8,128]{2,1,0:T(8,128)(2,1)S(1)}, u32[]{:S(2)}, u32[]{:S(2)}) async-start(bf16[64,8,128]{2,1,0:T(8,128)(2,1)} %shard_map.153), calls=%async_computation.5 | async-start | bytes 262144 | tf_op jit(solution)/shard_map/all_to_all | solution.py:19
  136.2 36.7 %copy-start.9 = (bf16[8,96]{1,0:T(8,128)(2,1)}, bf16[8,96]{1,0:T(8,128)(2,1)S(1)}, u32[]{:S(2)}) copy-start(bf16[8,96]{1,0:T(8,128)(2,1)S(1)} %get-tuple-element.47.vo_ref.refs_1_) | copy-start | bytes 4612
  136.2 17.4 %all-to-all-start.6 = ((bf16[64,8,128]{2,1,0:T(8,128)(2,1)}), bf16[64,8,128]{2,1,0:T(8,128)(2,1)S(1)}, u32[]{:S(2)}, u32[]{:S(2)}) async-start(bf16[64,8,128]{2,1,0:T(8,128)(2,1)} %get-tuple-element.43), calls=%async_computation.6 | async-start | bytes 262144 | tf_op jit(solution)/shard_map/all_to_all | solution.py:19
  142.1 30.9 %copy-start.5 = (f32[8,16]{1,0:T(8,128)}, f32[8,16]{1,0:T(8,128)S(1)}, u32[]{:S(2)}) copy-start(f32[8,16]{1,0:T(8,128)S(1)} %get-tuple-element.49.admit_ref.refs_3_) | copy-start | bytes 1540
  142.1 30.9 %copy-start.6 = (f32[8,16]{1,0:T(8,128)}, f32[8,16]{1,0:T(8,128)S(1)}, u32[]{:S(2)}) copy-start(f32[8,16]{1,0:T(8,128)S(1)} %get-tuple-element.48.retain_ref.refs_2_) | copy-start | bytes 1540
  153.6 19.4 %copy-start.1 = (bf16[64,8,128]{2,1,0:T(8,128)(2,1)}, bf16[64,8,128]{2,1,0:T(8,128)(2,1)S(1)}, u32[]{:S(2)}) copy-start(bf16[64,8,128]{2,1,0:T(8,128)(2,1)S(1)} %all-to-all-done.6.pieces_ref.refs_0_) | copy-start | bytes 393220
  154.7 17.3 %all-to-all-start.7 = ((bf16[64,8,128]{2,1,0:T(8,128)(2,1)}), bf16[64,8,128]{2,1,0:T(8,128)(2,1)S(1)}, u32[]{:S(2)}, u32[]{:S(2)}) async-start(bf16[64,8,128]{2,1,0:T(8,128)(2,1)} %shard_map.155), calls=%async_computation.7 | async-start | bytes 262144 | tf_op jit(solution)/shard_map/all_to_all | solution.py:19
  173.0 17.3 %all-to-all-start.8 = ((bf16[64,8,128]{2,1,0:T(8,128)(2,1)}), bf16[64,8,128]{2,1,0:T(8,128)(2,1)S(1)}, u32[]{:S(2)}, u32[]{:S(2)}) async-start(bf16[64,8,128]{2,1,0:T(8,128)(2,1)} %shard_map.156), calls=%async_computation.8 | async-start | bytes 262144 | tf_op jit(solution)/shard_map/all_to_all | solution.py:19
